TPU v7x, 32 devices: a whole 2x2x4 slice. The times are simulated.
32 devices in a mesh: grp: 2 (over y), st: 4 (over z), tp: 4 (over x, core).
Axes of the slice: x: 2, y: 2, z: 4, core: 2. Of those that a mesh axis runs over, the one named last changes fastest.
Arguments:
- tokens: bfloat16 [8192, 2048], P(('grp', 'st'), 'tp'), parts along dimension 0, may hold values from -6 to 6
- norm_gain: float32 [2048], replicated, may hold values from 0.1 to 1.9
- pool_weight: bfloat16 [4, 512, 512], P('tp'), may hold values from -0.25 to 0.25
- pool_scale: float32 [2048], P('tp'), may hold values from 0.1 to 1.9
- query_weight: bfloat16 [2048, 1024], P(None, 'tp'), may hold values from -3 to 3
- gate_weight: bfloat16 [2048, 8], replicated, may hold values from -0.125 to 0.125
- key_weight: bfloat16 [2048, 1024], P(None, 'tp'), may hold values from -0.125 to 0.125
- value_weight: bfloat16 [2048, 1024], P(None, 'tp'), may hold values from -0.125 to 0.125
- out_weight: bfloat16 [1024, 2048], P(None, 'tp'), may hold values from -0.1875 to 0.1875
- passage_gain: float32 [2048], replicated, may hold values from 0.1 to 1.9
- passage_store: bfloat16 [192, 64, 2048], P(('grp', 'st')), parts along dimension 0, may hold values from -6 to 6
- passage_ids: int32 [64, 4], P(('grp', 'st')), parts along dimension 0, may hold values from 0 to 95, as said below
Outputs:
- mixed: bfloat16 [8192, 2048], P(('grp', 'st'), 'tp'), parts along dimension 0
There are 2 independent parts, one for each index of `grp`. A program takes and returns all parts, laid end to end along the dimension named above; an argument that names none is the same for every part. Nothing has to cross between parts.
Inputs may be any that keep to these rules, and one draw needn't show every extreme that they name: `passage_ids`: the ids of the blocks of one index of st name at most 8 passages held by any one index of st, and exactly 8 held by some index.
All inputs are finite; a program needn't handle non-finite values.
Results may differ from a plain program's by a relative error of at most 0.009.
Values may be sent and summed in bfloat16 or wider, within the bound.
A program may use at most 128 MiB of HBM per device.

v0:
```python
import jax
import jax.numpy as jnp
from jax import lax
from jax.sharding import PartitionSpec as P

HD = 128
GROUPS = 4
SEQ_LEN = 256
BLK = 128
NPB = 4
PLEN = 64
P_DEV = 24
epsilon = 1e-06


def normalize_rows(fetched, passage_gain):
    wide_rows = fetched.astype(jnp.float32)
    inverse = lax.rsqrt(jnp.mean(wide_rows * wide_rows, axis=-1, keepdims=True) + epsilon)
    return (wide_rows * inverse * passage_gain).astype(jnp.bfloat16)


def project_rows(fetched, passage_gain, both_weights):
    count_rows = fetched.shape[0]
    flat_rows = normalize_rows(fetched.reshape(count_rows * PLEN, fetched.shape[2]), passage_gain)
    projected = jnp.dot(flat_rows, both_weights, preferred_element_type=jnp.float32).astype(
        jnp.bfloat16
    )
    return projected.reshape(count_rows, PLEN, both_weights.shape[1])


def per_device(
    tokens,
    norm_gain,
    pool_weight,
    pool_scale,
    query_weight,
    gate_weight,
    key_weight,
    value_weight,
    out_weight,
    passage_gain,
    passage_store,
    passage_ids,
):
    head_index = lax.axis_index("tp")
    tok_rows, width_local = tokens.shape
    full_width = width_local * lax.axis_size("tp")
    local_heads = query_weight.shape[1] // HD
    head_width = local_heads * HD
    wide_tokens = tokens.astype(jnp.float32)
    square_sums = lax.psum(jnp.sum(wide_tokens * wide_tokens, axis=1), "tp")
    inverse = lax.rsqrt(square_sums / full_width + epsilon)
    gain_local = lax.dynamic_slice_in_dim(norm_gain, head_index * width_local, width_local)
    normed = (wide_tokens * inverse[:, None] * gain_local[None, :]).astype(jnp.bfloat16)
    sequences = tok_rows // SEQ_LEN
    widest = 2**GROUPS
    window = jnp.left_shift(jnp.int32(2), head_index)
    grouped = normed.astype(jnp.float32).reshape(sequences, SEQ_LEN, width_local)
    running = jnp.cumsum(grouped, axis=1)
    padded = jnp.concatenate(
        [jnp.zeros((sequences, widest, width_local), jnp.float32), running], axis=1
    )
    lagged = lax.dynamic_slice_in_dim(padded, widest - window, SEQ_LEN, axis=1)
    position = jnp.arange(SEQ_LEN, dtype=jnp.int32)
    divisor = jnp.minimum(position + 1, window).astype(jnp.float32)
    pooled = (
        ((running - lagged) / divisor[None, :, None] - grouped)
        .astype(jnp.bfloat16)
        .reshape(tok_rows, width_local)
    )
    mixing = (
        jnp.dot(pooled, pool_weight[0], preferred_element_type=jnp.float32) * pool_scale[None, :]
    )
    gate_columns = lax.dynamic_slice_in_dim(
        gate_weight, head_index * local_heads, local_heads, axis=1
    )
    columns = lax.all_gather(normed, "tp", axis=1, tiled=True)
    query_sum = jnp.dot(columns, query_weight, preferred_element_type=jnp.float32)
    gate_sum = jnp.dot(columns, gate_columns, preferred_element_type=jnp.float32)
    queries = query_sum.astype(jnp.bfloat16)
    gating = jax.nn.sigmoid(gate_sum)
    flat_ids = passage_ids.reshape(-1)
    asked_count = flat_ids.shape[0]
    st_count = lax.axis_size("st")
    capacity = max(2, (asked_count + st_count - 1) // st_count)
    owners = flat_ids // P_DEV
    local_index = flat_ids % P_DEV
    order_index = jnp.arange(asked_count, dtype=jnp.int32)
    earlier = (owners[None, :] == owners[:, None]) & (order_index[None, :] < order_index[:, None])
    slot_index = jnp.sum(earlier.astype(jnp.int32), axis=1)
    position_flat = owners * capacity + slot_index
    slot_range = jnp.arange(st_count * capacity, dtype=jnp.int32)
    request_table = jnp.sum(
        jnp.where(position_flat[None, :] == slot_range[:, None], local_index[None, :], 0), axis=1
    )
    request_table = request_table.reshape(st_count, capacity)
    asked = lax.all_to_all(request_table, "st", split_axis=0, concat_axis=0, tiled=True)
    both_weights = jnp.concatenate([key_weight, value_weight], axis=1)
    projected_store = project_rows(passage_store, passage_gain, both_weights)
    projected = jnp.take(projected_store, asked.reshape(-1), axis=0)
    returned = lax.all_to_all(
        projected.reshape(st_count, capacity * PLEN, 2 * head_width),
        "st",
        split_axis=0,
        concat_axis=0,
        tiled=True,
    )
    key_values = jnp.take(
        returned.reshape(st_count * capacity, PLEN, 2 * head_width), position_flat, axis=0
    )
    block_count = tok_rows // BLK
    key_values = key_values.reshape(block_count, NPB * PLEN, 2 * head_width)
    key_rows = key_values[:, :, :head_width].reshape(block_count, NPB * PLEN, local_heads, HD)
    values = key_values[:, :, head_width:].reshape(block_count, NPB * PLEN, local_heads, HD)
    query_blocks = queries.reshape(block_count, BLK, local_heads, HD)
    scores = jnp.einsum(
        "bqhd,bkhd->bhqk", query_blocks, key_rows, preferred_element_type=jnp.float32
    ) * HD ** (-0.5)
    row_max = jnp.max(scores, axis=-1, keepdims=True)
    weights = jnp.exp(scores - row_max)
    probabilities = (weights / jnp.sum(weights, axis=-1, keepdims=True)).astype(jnp.bfloat16)
    attended = jnp.einsum(
        "bhqk,bkhd->bqhd", probabilities, values, preferred_element_type=jnp.float32
    ).reshape(tok_rows, local_heads, HD)
    head_out = (attended * gating[:, :, None]).astype(jnp.bfloat16).reshape(tok_rows, head_width)
    crossed = jnp.dot(
        lax.all_gather(head_out, "tp", axis=1, tiled=True),
        out_weight,
        preferred_element_type=jnp.float32,
    )
    return (mixing + crossed).astype(jnp.bfloat16)


def solution(mesh):
    in_specs = (
        P(("grp", "st"), "tp"),
        P(),
        P("tp", None, None),
        P("tp"),
        P(None, "tp"),
        P(),
        P(None, "tp"),
        P(None, "tp"),
        P(None, "tp"),
        P(),
        P(("grp", "st"), None, None),
        P(("grp", "st"), None),
    )
    out_specs = P(("grp", "st"), "tp")
    return jax.shard_map(
        per_device, mesh=mesh, in_specs=in_specs, out_specs=out_specs, check_vma=False
    )
```

profile of v0, /device:TPU:0, one launch (start us, length us, event | category | flops | bytes accessed | tf_op | source)
XLA Modules:
  0.0 155.8 jit_solution(16865734827480352059)
XLA Ops:
  6.5 0.8 copy.41
  7.4 0.1 ne.86
  7.5 0.1 rem.47
  7.6 0.1 div.68
  7.7 0.2 convert_reduce_fusion
  7.9 0.1 select_reduce_fusion
  8.0 0.7 all_to_all.9
  8.6 6.3 %all-to-all-start = ((s32[4,1,8]{2,1,0:T(1,128)}), s32[4,1,8]{2,1,0:T(1,128)S(1)}, u32[]{:S(2)}, u32[]{:S(2)}) async-start(s32[4,1,8]{2,1,0:T(1,128)} %bitcast.9), calls=%async_computation | async-start | bytes 4096 | tf_op jit(solution)/shard_map/all_to_all | solution.py:97
  15.0 1.5 fusion.6
  16.5 6.5 %psum.7 = f32[1024]{0:T(1024)S(1)} all-reduce(f32[1024]{0:T(1024)S(1)} %fusion.6), channel_id=1, replica_groups=mesh['grp'=2,'st'=4,'tp'=4] {'tp'}, use_global_device_ids=true, to_apply=%region_1.0 | all-reduce | flops 1024 | bytes 8192 | tf_op jit(solution)/shard_map/psum | solution.py:51
  23.0 0.8 dynamic_slice.9
  23.8 2.5 %fusion.8 = bf16[1024,512]{1,0:T(8,128)(2,1)} fusion(bf16[1024,512]{1,0:T(8,128)(2,1)} %param.12, f32[512]{0:T(512)S(1)} %dynamic_slice.9, f32[1024]{0:T(1024)S(1)} %add_rsqrt_fusion.1), kind=kLoop, calls=%fused_computation.16 | loop fusion | flops 2097152 | bytes 2103296 | tf_op jit(solution)/shard_map/convert_element_type | solution.py:54
  26.4 4.1 %multiply_reduce_fusion = f32[24,64]{1,0:T(8,128)S(1)} fusion(bf16[24,64,2048]{2,1,0:T(8,128)(2,1)} %param.22), kind=kLoop, calls=%fused_computation.6 | loop fusion | flops 9435648 | bytes 6297600 | tf_op jit(solution)/shard_map/reduce_sum | solution.py:18
  30.5 4.6 %fusion.2 = bf16[1536,2048]{1,0:T(8,128)(2,1)S(1)} fusion(f32[2048]{0:T(1024)S(1)} %copy-done.4, f32[1536]{0:T(1024)S(1)} %rsqrt.16, bf16[24,64,2048]{2,1,0:T(8,128)(2,1)} %param.22), kind=kLoop, calls=%fused_computation.5 | loop fusion | flops 12582912 | bytes 12597248 | tf_op jit(solution)/shard_map/convert_element_type | solution.py:19
  35.1 4.8 %convolution_convert_fusion = bf16[1536,512]{1,0:T(8,128)(2,1)} fusion(bf16[1536,2048]{1,0:T(8,128)(2,1)S(1)} %fusion.2, bf16[2048,256]{1,0:T(8,128)(2,1)S(1)} %copy-done.6, bf16[2048,256]{1,0:T(8,128)(2,1)S(1)} %copy-done.7), kind=kOutput, calls=%fused_computation.7 | convolution fusion | flops 3226206208 | bytes 9961472 | tf_op jit(solution)/shard_map/dot_general | solution.py:25
  39.9 0.5 broadcast.275
  40.4 0.7 reduce.4
  41.1 0.1 reshape.267
  41.3 0.1 broadcast_in_dim.63
  41.4 2.1 %gather_fusion = bf16[32,64,512]{2,1,0:T(8,128)(2,1)S(1)} fusion(bf16[24,64,512]{2,1,0:T(8,128)(2,1)} %bitcast.73, s32[1024]{0:T(1024)S(1)} %pad_clamp_fusion.1), kind=kCustom, calls=%fused_computation | custom fusion | bytes 4194432 | tf_op jit(solution)/shard_map/jit(_take)/gather | solution.py:100
  43.5 1.6 %bitcast_select_fusion.1 = bf16[4,512,512]{2,1,0:T(8,128)(2,1)} fusion(pred[4,512]{1,0:T(4,128)(4,1)S(1)} %broadcast_in_dim.63, bf16[4,512,512]{2,1,0:T(8,128)(2,1)S(1)} %bitcast.66), kind=kLoop, calls=%fused_computation.21 | loop fusion | flops 1048576 | bytes 4196352 | tf_op jit(solution)/shard_map/jit(_take)/select_n | solution.py:100
  45.1 4.5 %all-to-all-start.1 = ((bf16[4,512,512]{2,1,0:T(8,128)(2,1)}), bf16[4,512,512]{2,1,0:T(8,128)(2,1)S(1)}, u32[]{:S(2)}, u32[]{:S(2)}) async-start(bf16[4,512,512]{2,1,0:T(8,128)(2,1)} %bitcast_select_fusion.1), calls=%async_computation.1 | async-start | bytes 4194304 | tf_op jit(solution)/shard_map/all_to_all | solution.py:101
  49.8 0.1 and.63
  49.9 0.1 broadcast_in_dim.58
  50.1 47.4 %all-to-all-done.1 = bf16[4,512,512]{2,1,0:T(8,128)(2,1)S(1)} async-done(((bf16[4,512,512]{2,1,0:T(8,128)(2,1)}), bf16[4,512,512]{2,1,0:T(8,128)(2,1)S(1)}, u32[]{:S(2)}, u32[]{:S(2)}) %all-to-all-start.1) | async-done | bytes 2097184 | tf_op jit(solution)/shard_map/all_to_all | solution.py:101
  97.4 2.0 %gather_fusion.1 = bf16[32,64,512]{2,1,0:T(8,128)(2,1)} fusion(bf16[32,64,512]{2,1,0:T(8,128)(2,1)S(1)} %bitcast.65, s32[1024]{0:T(1024)S(1)} %pad_clamp_fusion), kind=kCustom, calls=%fused_computation.1 | custom fusion | bytes 4194432 | tf_op jit(solution)/shard_map/jit(_take)/gather | solution.py:108
  99.4 1.8 %bitcast_select_fusion = bf16[8,256,512]{2,1,0:T(8,128)(2,1)S(1)} fusion(pred[8,256]{1,0:T(8,128)(4,1)S(1)} %broadcast_in_dim.58, bf16[8,256,512]{2,1,0:T(8,128)(2,1)} %bitcast.67), kind=kLoop, calls=%fused_computation.20 | loop fusion | flops 1048576 | bytes 4196352 | tf_op jit(solution)/shard_map/jit(_take)/select_n | solution.py:108
  101.2 1.2 fusion.46
  102.4 1.5 copy.46
  103.9 1.3 copy.45
  105.2 3.7 %convolution_convert_fusion.1 = bf16[1024,256]{1,0:T(8,128)(2,1)S(1)} fusion(bf16[1024,2048]{1,0:T(8,128)(2,1)} %all-gather.3.cloned.1.call-done, bf16[2048,256]{1,0:T(8,128)(2,1)} %param.16), kind=kOutput, calls=%fused_computation.31 | convolution fusion | flops 1074003968 | bytes 5767168 | tf_op jit(solution)/shard_map/dot_general | solution.py:78
  108.9 0.1 reshape.270
  109.1 1.0 fusion.47
  110.1 1.8 %fusion.22 = f32[8,2,128,256]{3,2,1,0:T(8,128)} fusion(bf16[8,256,2,128]{1,3,2,0:T(8,128)(2,1)S(1)} %bitcast.70, bf16[8,128,2,128]{3,2,1,0:T(2,128)(2,1)S(1)} %reshape.270), kind=kOutput, calls=%fused_computation.41 | convolution fusion | flops 134217728 | bytes 3670016 | tf_op jit(solution)/shard_map/bqhd,bkhd->bhqk/dot_general | solution.py:116
  111.8 5.7 %convolution_bitcast_fusion = f32[8,128,2,128]{1,3,2,0:T(8,128)S(1)} fusion(bf16[8,256,2,128]{1,3,2,0:T(8,128)(2,1)} %bitcast.74, f32[8,2,128]{2,1,0:T(2,128)S(1)} %fusion.47, f32[8,2,128,256]{3,2,1,0:T(8,128)} %fusion.22), kind=kOutput, calls=%fused_computation.30 | convolution fusion | flops 136317184 | bytes 4202496 | tf_op jit(solution)/shard_map/bhqk,bkhd->bqhd/dot_general | solution.py:122
  117.5 0.6 copy.49
  118.1 3.4 %fusion.18 = f32[1024,2]{0,1:T(2,128)S(1)} fusion(bf16[1024,2048]{1,0:T(8,128)(2,1)} %all-gather.3.cloned.1.call-done, bf16[2048,8]{0,1:T(8,128)(2,1)} %param.17, s32[]{:T(128)S(6)} %select_n.108), kind=kOutput, calls=%fused_computation.35 | convolution fusion | flops 8394752 | bytes 4210692 | tf_op jit(solution)/shard_map/dot_general | solution.py:79
  121.5 1.0 fusion.19
  122.5 0.4 copy-done.1
  122.9 0.3 convert.2
  123.2 1.6 %fusion.12 = f32[4,512,2,128]{1,2,3,0:T(2,128)S(1)} fusion(f32[4,512,2,128]{1,3,2,0:T(8,128)S(1)} %bitcast.68), kind=kOutput, calls=%fused_computation.22 | output fusion | flops 66584576 | bytes 4194304 | tf_op jit(solution)/shard_map/reduce-window
  124.9 1.3 copy-done.2
  126.2 2.4 %broadcast_add_fusion = f32[4,512,2,128]{1,2,3,0:T(2,128)S(1)} fusion(f32[4,512,2,128]{1,2,3,0:T(2,128)} %copy-done.2, f32[4,512,2]{1,2,0:T(2,128)S(1)} %slice.21), kind=kLoop, calls=%fused_computation.39 | loop fusion | flops 524288 | bytes 4210688 | tf_op jit(solution)/shard_map/reduce_window_sum
  128.6 1.7 %copy.40 = f32[4,512,2,128]{1,3,2,0:T(8,128)} copy(f32[4,512,2,128]{1,2,3,0:T(2,128)S(1)} %broadcast_add_fusion) | data formatting | bytes 4194304 | tf_op jit(solution)/shard_map/reduce_window_sum
  130.3 3.1 %fusion.14 = bf16[4,256,512]{2,1,0:T(8,128)(2,1)S(1)} fusion(f32[4,256,512]{2,1,0:T(8,128)} %bitcast.64, s32[]{:T(128)S(6)} %select_n.96, f32[256]{0:T(256)S(1)} %minimum_convert_fusion, bf16[4,256,512]{2,1,0:T(8,128)(2,1)S(1)} %bitcast.63), kind=kLoop, calls=%fused_computation.27 | loop fusion | flops 2621440 | bytes 4195332 | tf_op jit(solution)/shard_map/convert_element_type | solution.py:68
  133.4 10.9 %all-gather.5.cloned.1.call-done = bf16[1024,1024]{0,1:T(8,128)(2,1)} async-done(((bf16[1024,256]{0,1:T(8,128)(2,1)}), bf16[1024,1024]{0,1:T(8,128)(2,1)}) %all-gather.5.cloned.1.call-update) | async-done | bytes 2097168 | tf_op jit(solution)/shard_map/all_gather | solution.py:127
  144.3 2.9 %fusion.50 = f32[1024,512]{1,0:T(8,128)S(1)} fusion(bf16[1024,1024]{0,1:T(8,128)(2,1)} %all-gather.5.cloned.1.call-done, bf16[1024,512]{1,0:T(8,128)(2,1)S(1)} %copy-done), kind=kOutput, calls=%fused_computation.83 | convolution fusion | flops 1073741824 | bytes 5242880 | tf_op jit(solution)/shard_map/dot_general | solution.py:126
  147.2 1.7 %add_convert_fusion = bf16[1024,512]{1,0:T(8,128)(2,1)} fusion(f32[1024,512]{1,0:T(8,128)S(1)} %fusion.50, bf16[1024,512]{1,0:T(8,128)(2,1)S(1)} %bitcast.71, f32[512]{0:T(512)S(1)} %copy-done.5, bf16[1,512,512]{2,1,0:T(8,128)(2,1)S(1)} %copy-done.3), kind=kOutput, calls=%fused_computation.24 | convolution fusion | flops 538443776 | bytes 4720640 | tf_op jit(solution)/shard_map/dot_general | solution.py:72
  (41 shorter events, 0.6 us)
Async XLA Ops:
  6.5 137.8 %copy-start = (bf16[1024,512]{1,0:T(8,128)(2,1)S(1)}, bf16[1024,512]{1,0:T(8,128)(2,1)}, u32[]{:S(2)}) copy-start(bf16[1024,512]{1,0:T(8,128)(2,1)} %param.20) | copy-start | bytes 3145732
  8.6 31.3 %all-to-all-start = ((s32[4,1,8]{2,1,0:T(1,128)}), s32[4,1,8]{2,1,0:T(1,128)S(1)}, u32[]{:S(2)}, u32[]{:S(2)}) async-start(s32[4,1,8]{2,1,0:T(1,128)} %bitcast.9), calls=%async_computation | async-start | bytes 4096 | tf_op jit(solution)/shard_map/all_to_all | solution.py:97
  15.0 90.2 %all-gather.3.cloned.1.call-start = ((), (), s32[]{:S(2)}) async-start(), calls=%async_computation.2 | async-start | bytes 5242880 | tf_op jit(solution)/shard_map/all_gather | solution.py:77
  26.3 4.2 %copy-start.4 = (f32[2048]{0:T(1024)S(1)}, f32[2048]{0:T(1024)}, u32[]{:S(2)}) copy-start(f32[2048]{0:T(1024)} %param.21) | copy-start | bytes 24580
  30.5 4.6 %copy-start.6 = (bf16[2048,256]{1,0:T(8,128)(2,1)S(1)}, bf16[2048,256]{1,0:T(8,128)(2,1)}, u32[]{:S(2)}) copy-start(bf16[2048,256]{1,0:T(8,128)(2,1)} %param.19) | copy-start | bytes 3145732
  30.5 4.6 %copy-start.7 = (bf16[2048,256]{1,0:T(8,128)(2,1)S(1)}, bf16[2048,256]{1,0:T(8,128)(2,1)}, u32[]{:S(2)}) copy-start(bf16[2048,256]{1,0:T(8,128)(2,1)} %param.18) | copy-start | bytes 3145732
  45.1 52.4 %all-to-all-start.1 = ((bf16[4,512,512]{2,1,0:T(8,128)(2,1)}), bf16[4,512,512]{2,1,0:T(8,128)(2,1)S(1)}, u32[]{:S(2)}, u32[]{:S(2)}) async-start(bf16[4,512,512]{2,1,0:T(8,128)(2,1)} %bitcast_select_fusion.1), calls=%async_computation.1 | async-start | bytes 4194304 | tf_op jit(solution)/shard_map/all_to_all | solution.py:101
  49.6 94.7 %all-gather.5.cloned.1.call-start = ((), (), s32[]{:S(2)}) async-start(), calls=%async_computation.3 | async-start | bytes 2621440 | tf_op jit(solution)/shard_map/all_gather | solution.py:127
  121.5 1.4 copy-start.1
  124.9 1.3 copy-start.2
  133.4 13.9 %copy-start.3 = (bf16[1,512,512]{2,1,0:T(8,128)(2,1)S(1)}, bf16[1,512,512]{2,1,0:T(8,128)(2,1)}, u32[]{:S(2)}) copy-start(bf16[1,512,512]{2,1,0:T(8,128)(2,1)} %param.14) | copy-start | bytes 1572868
  133.4 13.9 %copy-start.5 = (f32[512]{0:T(512)S(1)}, f32[512]{0:T(512)}, u32[]{:S(2)}) copy-start(f32[512]{0:T(512)} %param.15) | copy-start | bytes 6148
Sparse Core Ops, SparseCore 0:
  26.5 35.3 all-gather.2
  122.6 21.6 all-gather.4
where the time goes:
time: 156 us
  waiting for transfers between devices  58.3 us (37%)
  other arithmetic  25.5 us (16%)
  matrix products  24.9 us (16%)
  local copies, waits for them, and re-layouts  16 us (10%)
  between operations  13.6 us (9%)
  starting transfers between devices  10.9 us (7%)
  blocking collectives  6.52 us (4%)
    all_to_all x1, waiting for transfers between devices, per_device(): lax.all_to_all(projected.reshape(st_count, capacity * PLEN, 2 * head_widt...  47.4 us
    all_gather x1, waiting for transfers between devices, per_device(): lax.all_gather(head_out, 'tp', axis=1, tiled=True)  10.9 us
    psum x1, blocking collectives, per_device(): square_sums = lax.psum(jnp.sum(wide_tokens * wide_tokens, axis=1), 'tp')  6.52 us
    all_to_all x1, starting transfers between devices, per_device(): lax.all_to_all(request_table, 'st', split_axis=0, concat_axis=0, tiled=True)  6.35 us
    dot_general x1, matrix products, per_device(): jnp.einsum('bhqk,bkhd->bqhd', probabilities, values, preferred_element_ty...  5.65 us
    dot_general x1, matrix products, project_rows(): jnp.dot(flat_rows, both_weights, preferred_element_type=jnp.float32)  4.79 us
    convert_element_type x1, other arithmetic, normalize_rows(): return (wide_rows * inverse * passage_gain).astype(jnp.bfloat16)  4.56 us
    all_to_all x1, starting transfers between devices, per_device(): lax.all_to_all(projected.reshape(st_count, capacity * PLEN, 2 * head_widt...  4.53 us
  transfers between devices with their start and end apart: 4, of which 2 were waited for; matrix products, arithmetic and copies ran while one was open for 26% of the time, Pallas kernels for 0%

commit v1 on v0

--- a/solution.py
+++ b/solution.py
@@ -124,7 +124,7 @@
     ).reshape(tok_rows, local_heads, HD)
     head_out = (attended * gating[:, :, None]).astype(jnp.bfloat16).reshape(tok_rows, head_width)
     crossed = jnp.dot(
-        lax.all_gather(head_out, "tp", axis=1, tiled=True),
+        jnp.concatenate(lax.all_gather(head_out, "tp"), axis=1),
         out_weight,
         preferred_element_type=jnp.float32,
     )

time: 156 us -> 163 us (1.045)
  local copies, waits for them, and re-layouts: 16 us -> 21.8 us
    all_gather x0 -> x1, local copies, waits for them, and re-layouts: none -> 3.96 us  [per_device(): lax.all_gather(head_out, 'tp')]
    convert_element_type x0 -> x1, local copies, waits for them, and re-layouts: none -> 2.04 us  [per_device(): (attended * gating[:, :, None]).astype(jnp.bfloat16)]
  transfers between devices with their start and end apart: 4 -> 4, of which waited for: 2 -> 2; matrix products, arithmetic and copies ran while one was open for 26% -> 25% of each run, Pallas kernels for 0% -> 0%
where the time goes in v1:
time: 163 us; the launch traced here: 162 us
  waiting for transfers between devices  58.8 us (36%)
  other arithmetic  25.3 us (16%)
  matrix products  25 us (15%)
  local copies, waits for them, and re-layouts  21.8 us (13%)
  between operations  13.6 us (8%)
  starting transfers between devices  10.9 us (7%)
  blocking collectives  6.52 us (4%)
    all_to_all x1, waiting for transfers between devices, per_device(): lax.all_to_all(projected.reshape(st_count, capacity * PLEN, 2 * head_widt...  47.4 us
    all_gather x1, waiting for transfers between devices, per_device(): lax.all_gather(head_out, 'tp')  11.4 us
    psum x1, blocking collectives, per_device(): square_sums = lax.psum(jnp.sum(wide_tokens * wide_tokens, axis=1), 'tp')  6.52 us
    all_to_all x1, starting transfers between devices, per_device(): lax.all_to_all(request_table, 'st', split_axis=0, concat_axis=0, tiled=True)  6.35 us
    dot_general x1, matrix products, per_device(): jnp.einsum('bhqk,bkhd->bqhd', probabilities, values, preferred_element_ty...  5.65 us
    dot_general x1, matrix products, project_rows(): jnp.dot(flat_rows, both_weights, preferred_element_type=jnp.float32)  4.79 us
    convert_element_type x1, other arithmetic, normalize_rows(): return (wide_rows * inverse * passage_gain).astype(jnp.bfloat16)  4.56 us
    all_to_all x1, starting transfers between devices, per_device(): lax.all_to_all(projected.reshape(st_count, capacity * PLEN, 2 * head_widt...  4.53 us
  transfers between devices with their start and end apart: 4, of which 2 were waited for; matrix products, arithmetic and copies ran while one was open for 25% of the time, Pallas kernels for 0%

profile of v1, /device:TPU:0, one launch (start us, length us, event | category | flops | bytes accessed | tf_op | source)
XLA Modules:
  0.0 161.9 jit_solution(18299036360403414874)
XLA Ops:
  6.5 0.8 copy.43
  7.4 0.1 ne.86
  7.7 0.2 convert_reduce_fusion
  7.9 0.1 select_reduce_fusion
  8.0 0.7 all_to_all.9
  8.6 6.3 %all-to-all-start = ((s32[4,1,8]{2,1,0:T(1,128)}), s32[4,1,8]{2,1,0:T(1,128)S(1)}, u32[]{:S(2)}, u32[]{:S(2)}) async-start(s32[4,1,8]{2,1,0:T(1,128)} %bitcast.9), calls=%async_computation | async-start | bytes 4096 | tf_op jit(solution)/shard_map/all_to_all | solution.py:97
  15.0 1.5 fusion.6
  16.5 6.5 %psum.7 = f32[1024]{0:T(1024)S(1)} all-reduce(f32[1024]{0:T(1024)S(1)} %fusion.6), channel_id=1, replica_groups=mesh['grp'=2,'st'=4,'tp'=4] {'tp'}, use_global_device_ids=true, to_apply=%region_1.0 | all-reduce | flops 1024 | bytes 8192 | tf_op jit(solution)/shard_map/psum | solution.py:51
  23.0 0.8 dynamic_slice.9
  23.8 2.5 %fusion.8 = bf16[1024,512]{1,0:T(8,128)(2,1)} fusion(bf16[1024,512]{1,0:T(8,128)(2,1)} %param.12, f32[512]{0:T(512)S(1)} %dynamic_slice.9, f32[1024]{0:T(1024)S(1)} %add_rsqrt_fusion.1), kind=kLoop, calls=%fused_computation.16 | loop fusion | flops 2097152 | bytes 2103296 | tf_op jit(solution)/shard_map/convert_element_type | solution.py:54
  26.4 4.1 %multiply_reduce_fusion = f32[24,64]{1,0:T(8,128)S(1)} fusion(bf16[24,64,2048]{2,1,0:T(8,128)(2,1)} %param.22), kind=kLoop, calls=%fused_computation.6 | loop fusion | flops 9435648 | bytes 6297600 | tf_op jit(solution)/shard_map/reduce_sum | solution.py:18
  30.5 4.6 %fusion.2 = bf16[1536,2048]{1,0:T(8,128)(2,1)S(1)} fusion(f32[2048]{0:T(1024)S(1)} %copy-done.4, f32[1536]{0:T(1024)S(1)} %rsqrt.16, bf16[24,64,2048]{2,1,0:T(8,128)(2,1)} %param.22), kind=kLoop, calls=%fused_computation.5 | loop fusion | flops 12582912 | bytes 12597248 | tf_op jit(solution)/shard_map/convert_element_type | solution.py:19
  35.1 4.8 %convolution_convert_fusion = bf16[1536,512]{1,0:T(8,128)(2,1)} fusion(bf16[1536,2048]{1,0:T(8,128)(2,1)S(1)} %fusion.2, bf16[2048,256]{1,0:T(8,128)(2,1)S(1)} %copy-done.6, bf16[2048,256]{1,0:T(8,128)(2,1)S(1)} %copy-done.7), kind=kOutput, calls=%fused_computation.7 | convolution fusion | flops 3226206208 | bytes 9961472 | tf_op jit(solution)/shard_map/dot_general | solution.py:25
  39.9 0.5 broadcast.276
  40.4 0.7 reduce.4
  41.1 0.1 reshape.292
  41.3 0.1 broadcast_in_dim.63
  41.4 2.1 %gather_fusion = bf16[32,64,512]{2,1,0:T(8,128)(2,1)S(1)} fusion(bf16[24,64,512]{2,1,0:T(8,128)(2,1)} %bitcast.73, s32[1024]{0:T(1024)S(1)} %pad_clamp_fusion.1), kind=kCustom, calls=%fused_computation | custom fusion | bytes 4194432 | tf_op jit(solution)/shard_map/jit(_take)/gather | solution.py:100
  43.5 1.6 bitcast_select_fusion.1
  45.1 4.5 %all-to-all-start.1 = ((bf16[4,512,512]{2,1,0:T(8,128)(2,1)}), bf16[4,512,512]{2,1,0:T(8,128)(2,1)S(1)}, u32[]{:S(2)}, u32[]{:S(2)}) async-start(bf16[4,512,512]{2,1,0:T(8,128)(2,1)} %bitcast_select_fusion.1), calls=%async_computation.1 | async-start | bytes 4194304 | tf_op jit(solution)/shard_map/all_to_all | solution.py:101
  49.8 0.1 and.63
  49.9 0.1 broadcast_in_dim.58
  50.1 47.4 %all-to-all-done.1 = bf16[4,512,512]{2,1,0:T(8,128)(2,1)S(1)} async-done(((bf16[4,512,512]{2,1,0:T(8,128)(2,1)}), bf16[4,512,512]{2,1,0:T(8,128)(2,1)S(1)}, u32[]{:S(2)}, u32[]{:S(2)}) %all-to-all-start.1) | async-done | bytes 2097184 | tf_op jit(solution)/shard_map/all_to_all | solution.py:101
  97.4 2.0 %gather_fusion.1 = bf16[32,64,512]{2,1,0:T(8,128)(2,1)} fusion(bf16[32,64,512]{2,1,0:T(8,128)(2,1)S(1)} %bitcast.66, s32[1024]{0:T(1024)S(1)} %pad_clamp_fusion), kind=kCustom, calls=%fused_computation.1 | custom fusion | bytes 4194432 | tf_op jit(solution)/shard_map/jit(_take)/gather | solution.py:108
  99.4 1.8 %bitcast_select_fusion = bf16[8,256,512]{2,1,0:T(8,128)(2,1)S(1)} fusion(pred[8,256]{1,0:T(8,128)(4,1)S(1)} %broadcast_in_dim.58, bf16[8,256,512]{2,1,0:T(8,128)(2,1)} %bitcast.68), kind=kLoop, calls=%fused_computation.20 | loop fusion | flops 1048576 | bytes 4196352 | tf_op jit(solution)/shard_map/jit(_take)/select_n | solution.py:108
  101.2 1.2 fusion.46
  102.4 1.5 copy.48
  103.9 1.3 copy.47
  105.2 3.7 %convolution_convert_fusion.1 = bf16[1024,256]{1,0:T(8,128)(2,1)S(1)} fusion(bf16[1024,2048]{1,0:T(8,128)(2,1)} %all-gather.3.cloned.1.call-done, bf16[2048,256]{1,0:T(8,128)(2,1)} %param.16), kind=kOutput, calls=%fused_computation.31 | convolution fusion | flops 1074003968 | bytes 5767168 | tf_op jit(solution)/shard_map/dot_general | solution.py:78
  108.9 0.1 reshape.295
  109.1 1.0 fusion.47
  110.1 1.8 %fusion.22 = f32[8,2,128,256]{3,2,1,0:T(8,128)} fusion(bf16[8,256,2,128]{1,3,2,0:T(8,128)(2,1)S(1)} %bitcast.71, bf16[8,128,2,128]{3,2,1,0:T(2,128)(2,1)S(1)} %reshape.295), kind=kOutput, calls=%fused_computation.41 | convolution fusion | flops 134217728 | bytes 3670016 | tf_op jit(solution)/shard_map/bqhd,bkhd->bhqk/dot_general | solution.py:116
  111.8 5.7 %convolution_bitcast_fusion = f32[8,128,2,128]{1,3,2,0:T(8,128)S(1)} fusion(bf16[8,256,2,128]{1,3,2,0:T(8,128)(2,1)} %bitcast.75, f32[8,2,128]{2,1,0:T(2,128)S(1)} %fusion.47, f32[8,2,128,256]{3,2,1,0:T(8,128)} %fusion.22), kind=kOutput, calls=%fused_computation.30 | convolution fusion | flops 136317184 | bytes 4202496 | tf_op jit(solution)/shard_map/bhqk,bkhd->bqhd/dot_general | solution.py:122
  117.5 0.6 copy.51
  118.1 0.2 reshape.297
  118.3 3.4 %fusion.18 = f32[1024,2]{0,1:T(2,128)S(1)} fusion(bf16[1024,2048]{1,0:T(8,128)(2,1)} %all-gather.3.cloned.1.call-done, bf16[2048,8]{0,1:T(8,128)(2,1)} %param.17, s32[]{:T(128)S(6)} %select_n.108), kind=kOutput, calls=%fused_computation.35 | convolution fusion | flops 8394752 | bytes 4210692 | tf_op jit(solution)/shard_map/dot_general | solution.py:79
  121.7 0.9 fusion.19
  122.6 2.0 %copy.52 = bf16[1,1024,256]{2,1,0:T(8,128)(2,1)} copy(bf16[1,1024,256]{1,2,0:T(8,128)(2,1)} %fusion.19) | data formatting | bytes 1048576 | tf_op jit(solution)/shard_map/convert_element_type | solution.py:125
  124.7 0.3 convert.2
  124.9 1.6 %fusion.12 = f32[4,512,2,128]{1,2,3,0:T(2,128)S(1)} fusion(f32[4,512,2,128]{1,3,2,0:T(8,128)S(1)} %bitcast.69), kind=kOutput, calls=%fused_computation.22 | output fusion | flops 66584576 | bytes 4194304 | tf_op jit(solution)/shard_map/reduce-window
  126.6 1.3 copy-done.2
  128.0 2.3 %broadcast_add_fusion = f32[4,512,2,128]{1,2,3,0:T(2,128)S(1)} fusion(f32[4,512,2,128]{1,2,3,0:T(2,128)} %copy-done.2, f32[4,512,2]{1,2,0:T(2,128)S(1)} %slice.21), kind=kLoop, calls=%fused_computation.39 | loop fusion | flops 524288 | bytes 4210688 | tf_op jit(solution)/shard_map/reduce_window_sum
  130.3 1.7 %copy.42 = f32[4,512,2,128]{1,3,2,0:T(8,128)} copy(f32[4,512,2,128]{1,2,3,0:T(2,128)S(1)} %broadcast_add_fusion) | data formatting | bytes 4194304 | tf_op jit(solution)/shard_map/reduce_window_sum
  132.0 3.1 %fusion.14 = bf16[4,256,512]{2,1,0:T(8,128)(2,1)S(1)} fusion(f32[4,256,512]{2,1,0:T(8,128)} %bitcast.65, s32[]{:T(128)S(6)} %select_n.96, f32[256]{0:T(256)S(1)} %minimum_convert_fusion, bf16[4,256,512]{2,1,0:T(8,128)(2,1)S(1)} %bitcast.64), kind=kLoop, calls=%fused_computation.27 | loop fusion | flops 2621440 | bytes 4195332 | tf_op jit(solution)/shard_map/convert_element_type | solution.py:68
  135.0 11.4 %all-gather.5.cloned.1.call-done = bf16[4,1024,256]{2,1,0:T(8,128)(2,1)} async-done(((bf16[1,1024,256]{2,1,0:T(8,128)(2,1)}), bf16[4,1024,256]{2,1,0:T(8,128)(2,1)}) %all-gather.5.cloned.1.call-update) | async-done | bytes 2097168 | tf_op jit(solution)/shard_map/all_gather | solution.py:127
  146.5 4.0 %copy.53 = bf16[4,1024,256]{1,2,0:T(8,128)(2,1)} copy(bf16[4,1024,256]{2,1,0:T(8,128)(2,1)} %all-gather.5.cloned.1.call-done) | data formatting | bytes 4194304 | tf_op jit(solution)/shard_map/all_gather | solution.py:127
  150.4 2.9 %fusion.50 = f32[1024,512]{1,0:T(8,128)S(1)} fusion(bf16[1024,1024]{0,1:T(8,128)(2,1)} %bitcast.74, bf16[1024,512]{1,0:T(8,128)(2,1)S(1)} %copy-done), kind=kOutput, calls=%fused_computation.83 | convolution fusion | flops 1073741824 | bytes 5242880 | tf_op jit(solution)/shard_map/dot_general | solution.py:126
  153.4 1.7 %add_convert_fusion = bf16[1024,512]{1,0:T(8,128)(2,1)} fusion(f32[1024,512]{1,0:T(8,128)S(1)} %fusion.50, bf16[1024,512]{1,0:T(8,128)(2,1)S(1)} %bitcast.72, f32[512]{0:T(512)S(1)} %copy-done.5, bf16[1,512,512]{2,1,0:T(8,128)(2,1)S(1)} %copy-done.3), kind=kOutput, calls=%fused_computation.24 | convolution fusion | flops 538443776 | bytes 4720640 | tf_op jit(solution)/shard_map/dot_general | solution.py:72
  (44 shorter events, 0.8 us)
Async XLA Ops:
  6.5 143.9 %copy-start = (bf16[1024,512]{1,0:T(8,128)(2,1)S(1)}, bf16[1024,512]{1,0:T(8,128)(2,1)}, u32[]{:S(2)}) copy-start(bf16[1024,512]{1,0:T(8,128)(2,1)} %param.20) | copy-start | bytes 3145732
  8.6 31.3 %all-to-all-start = ((s32[4,1,8]{2,1,0:T(1,128)}), s32[4,1,8]{2,1,0:T(1,128)S(1)}, u32[]{:S(2)}, u32[]{:S(2)}) async-start(s32[4,1,8]{2,1,0:T(1,128)} %bitcast.9), calls=%async_computation | async-start | bytes 4096 | tf_op jit(solution)/shard_map/all_to_all | solution.py:97
  15.0 90.2 %all-gather.3.cloned.1.call-start = ((), (), s32[]{:S(2)}) async-start(), calls=%async_computation.2 | async-start | bytes 5242880 | tf_op jit(solution)/shard_map/all_gather | solution.py:77
  26.3 4.2 %copy-start.4 = (f32[2048]{0:T(1024)S(1)}, f32[2048]{0:T(1024)}, u32[]{:S(2)}) copy-start(f32[2048]{0:T(1024)} %param.21) | copy-start | bytes 24580
  30.5 4.6 %copy-start.6 = (bf16[2048,256]{1,0:T(8,128)(2,1)S(1)}, bf16[2048,256]{1,0:T(8,128)(2,1)}, u32[]{:S(2)}) copy-start(bf16[2048,256]{1,0:T(8,128)(2,1)} %param.19) | copy-start | bytes 3145732
  30.5 4.6 %copy-start.7 = (bf16[2048,256]{1,0:T(8,128)(2,1)S(1)}, bf16[2048,256]{1,0:T(8,128)(2,1)}, u32[]{:S(2)}) copy-start(bf16[2048,256]{1,0:T(8,128)(2,1)} %param.18) | copy-start | bytes 3145732
  45.1 52.4 %all-to-all-start.1 = ((bf16[4,512,512]{2,1,0:T(8,128)(2,1)}), bf16[4,512,512]{2,1,0:T(8,128)(2,1)S(1)}, u32[]{:S(2)}, u32[]{:S(2)}) async-start(bf16[4,512,512]{2,1,0:T(8,128)(2,1)} %bitcast_select_fusion.1), calls=%async_computation.1 | async-start | bytes 4194304 | tf_op jit(solution)/shard_map/all_to_all | solution.py:101
  49.6 96.9 %all-gather.5.cloned.1.call-start = ((), (), s32[]{:S(2)}) async-start(), calls=%async_computation.3 | async-start | bytes 2621440 | tf_op jit(solution)/shard_map/all_gather | solution.py:127
  121.7 3.0 %copy-start.1 = (bf16[1024,512]{1,0:T(8,128)(2,1)S(1)}, bf16[1024,512]{1,0:T(8,128)(2,1)}, u32[]{:S(2)}) copy-start(bf16[1024,512]{1,0:T(8,128)(2,1)} %fusion.8) | copy-start | bytes 3145732
  126.6 1.3 copy-start.2
  150.4 2.9 %copy-start.3 = (bf16[1,512,512]{2,1,0:T(8,128)(2,1)S(1)}, bf16[1,512,512]{2,1,0:T(8,128)(2,1)}, u32[]{:S(2)}) copy-start(bf16[1,512,512]{2,1,0:T(8,128)(2,1)} %param.14) | copy-start | bytes 1572868
  150.4 3.0 %copy-start.5 = (f32[512]{0:T(512)S(1)}, f32[512]{0:T(512)}, u32[]{:S(2)}) copy-start(f32[512]{0:T(512)} %param.15) | copy-start | bytes 6148
Sparse Core Ops, SparseCore 0:
  26.5 35.3 all-gather.2
  124.8 21.6 all-gather.4
